TPU v7x, 32 devices: a whole 2x2x4 slice. The times are simulated.
32 devices in a mesh: sp: 8 (over z, x), tp: 4 (over y, core).
Axes of the slice: x: 2, y: 2, z: 4, core: 2. Of those that a mesh axis runs over, the one named last changes fastest.
Arguments:
- queries: bfloat16 [4096, 512], P('sp', 'tp'), may hold values from -16 to 16
- key_heads: bfloat16 [4096, 512], P('sp', 'tp'), may hold values from -16 to 16
- value_heads: bfloat16 [4096, 512], P('sp', 'tp'), may hold values from -6 to 6
- head_gain: float32 [512], P('tp'), may hold values from 0.1 to 1.9
- residual: bfloat16 [4096, 2048], P(('sp', 'tp')), may hold values from -6 to 6
- out_weight: bfloat16 [512, 2048], replicated, may hold values from -0.25 to 0.25
- norm_gain: float32 [2048], replicated, may hold values from 0.1 to 1.9
- shared_gate: bfloat16 [2048, 512], replicated, may hold values from -0.125 to 0.125
- shared_up: bfloat16 [2048, 512], replicated, may hold values from -0.125 to 0.125
- shared_down: bfloat16 [512, 2048], replicated, may hold values from -0.25 to 0.25
- expert_gate: bfloat16 [64, 2048, 512], P(('sp', 'tp')), may hold values from -0.125 to 0.125
- expert_up: bfloat16 [64, 2048, 512], P(('sp', 'tp')), may hold values from -0.125 to 0.125
- expert_down: bfloat16 [64, 512, 2048], P(('sp', 'tp')), may hold values from -0.25 to 0.25
- routed_experts: int32 [4096, 4], P(('sp', 'tp')), may hold values from 0 to 63, all different within a row; in each aligned block of 128 rows (0 to 127, 128 to 255, ...) at most 12 rows name the same one
- route_weights: float32 [4096, 4], P(('sp', 'tp')), may hold values from 0.1 to 1.5
Outputs:
- layer_output: bfloat16 [4096, 2048], P(('sp', 'tp'))
Inputs may be any that keep to these rules, and one draw needn't show every extreme that they name: `routed_experts`: each row names 4 different experts. Within the rows of one device (128 consecutive rows, aligned) no expert is named more than 12 times, and in every draw some expert is named exactly 12 times in some device's rows.
All inputs are finite; a program needn't handle non-finite values.
Results may differ from a plain program's by a relative error of at most 0.014.
Values may be sent and summed in bfloat16 or wider, within the bound.
A program may use at most 128 MiB of HBM per device.

v0:
```python
import math
import jax
import jax.numpy as jnp
from jax import lax
from jax.sharding import PartitionSpec as P

HEAD_DIM = 64
EPSILON = 1e-06


def block_terms(query_block, key_block, value_block, query_start, key_start):
    scale = 1.0 / math.sqrt(HEAD_DIM)
    scores = (
        jnp.einsum("qhd,khd->hqk", query_block, key_block, preferred_element_type=jnp.float32)
        * scale
    )
    query_places = query_start + lax.iota(jnp.int32, query_block.shape[0])
    key_places = key_start + lax.iota(jnp.int32, key_block.shape[0])
    earlier = (key_places[None, :] < query_places[:, None])[None]
    stay_log = jnp.where(earlier, jax.nn.log_sigmoid(-scores), 0.0)
    after_log = lax.cumsum(stay_log, axis=2, reverse=True) - stay_log
    weights = jnp.where(earlier, jnp.exp(jax.nn.log_sigmoid(scores) + after_log), 0.0).astype(
        jnp.bfloat16
    )
    partial_out = jnp.einsum(
        "hqk,khd->qhd", weights, value_block, preferred_element_type=jnp.float32
    )
    block_total = jnp.transpose(jnp.sum(stay_log, axis=2))
    return (block_total, partial_out)


def head_norm(mixed, head_gain):
    inverse = lax.rsqrt(jnp.mean(mixed * mixed, axis=2, keepdims=True) + EPSILON)
    normed = mixed * inverse * head_gain.reshape(mixed.shape[1], mixed.shape[2])
    return normed.reshape(mixed.shape[0], -1).astype(jnp.bfloat16)


def stick_breaking(queries, key_heads, value_heads):
    seq_count = queries.shape[0]
    head_count = queries.shape[1] // HEAD_DIM
    shard_count = lax.axis_size("sp")
    shard_place = lax.axis_index("sp")
    query_width = 512
    query_blocks = queries.reshape(seq_count // query_width, query_width, head_count, HEAD_DIM)
    block_starts = shard_place * seq_count + query_width * jnp.arange(
        seq_count // query_width, dtype=jnp.int32
    )

    def shard_terms(key_block, value_block, key_start):

        def one_block(inputs):
            query_block, query_start = inputs
            return block_terms(query_block, key_block, value_block, query_start, key_start)

        totals, partials = lax.map(one_block, (query_blocks, block_starts))
        return (
            totals.reshape(seq_count, head_count),
            partials.reshape(seq_count, head_count, HEAD_DIM),
        )

    initial = (
        jnp.zeros((shard_count, seq_count, head_count), jnp.float32),
        jnp.zeros((shard_count, seq_count, head_count, HEAD_DIM), jnp.float32),
    )
    key_piece = lax.all_gather(key_heads, "sp", axis=0, tiled=True).reshape(
        -1, seq_count, head_count, HEAD_DIM
    )
    value_piece = lax.all_gather(value_heads, "sp", axis=0, tiled=True).reshape(
        -1, seq_count, head_count, HEAD_DIM
    )

    def add_one(shard_step, state):
        total_store, partial_store = state
        key_block = lax.dynamic_index_in_dim(key_piece, shard_step, 0, keepdims=False)
        value_block = lax.dynamic_index_in_dim(value_piece, shard_step, 0, keepdims=False)

        def compute(unused):
            return shard_terms(key_block, value_block, shard_step * seq_count)

        def nothing(unused):
            return (
                jnp.zeros((seq_count, head_count), jnp.float32),
                jnp.zeros((seq_count, head_count, HEAD_DIM), jnp.float32),
            )

        totals, partials = lax.cond(shard_step <= shard_place, compute, nothing, 0)
        total_store = lax.dynamic_update_index_in_dim(total_store, totals, shard_step, 0)
        partial_store = lax.dynamic_update_index_in_dim(partial_store, partials, shard_step, 0)
        return (total_store, partial_store)

    totals, partials = lax.fori_loop(0, key_piece.shape[0], add_one, initial)
    later = lax.cumsum(totals, axis=0, reverse=True) - totals
    return jnp.sum(jnp.exp(later)[..., None] * partials, axis=0)


def routed_sum(expert_input, expert_gate, expert_up, expert_down, routed_experts, route_weights):
    row_count, pick_count = routed_experts.shape
    local_experts = expert_gate.shape[0]
    model_width = expert_input.shape[1]
    sp_count = lax.axis_size("sp")
    tp_count = lax.axis_size("tp")
    device_count = sp_count * tp_count
    expert_count = local_experts * device_count
    capacity = max(2, 3 * row_count * pick_count // (2 * expert_count))
    flat_experts = routed_experts.reshape(-1)
    expert_table = (
        flat_experts[:, None] == jnp.arange(expert_count, dtype=jnp.int32)[None, :]
    ).astype(jnp.int32)
    ranking = jnp.sum(jnp.cumsum(expert_table, axis=0) * expert_table, axis=1) - 1
    holder = flat_experts // local_experts
    resident = flat_experts % local_experts
    slot_index = (resident * device_count + holder) * capacity + ranking
    placement = (
        slot_index[:, None] == jnp.arange(expert_count * capacity, dtype=jnp.int32)[None, :]
    ).astype(jnp.bfloat16)
    token_place = jnp.sum(placement.reshape(row_count, pick_count, -1), axis=1)
    outgoing = jnp.einsum(
        "rs,rd->sd", token_place, expert_input, preferred_element_type=jnp.float32
    ).astype(jnp.bfloat16)
    outgoing = outgoing.reshape(local_experts, device_count, capacity, model_width)
    arrived = lax.all_to_all(outgoing, ("sp", "tp"), split_axis=1, concat_axis=1, tiled=True)
    grouped = arrived.reshape(local_experts, -1, model_width)
    gate_part = jnp.einsum("erd,edf->erf", grouped, expert_gate, preferred_element_type=jnp.float32)
    up_part = jnp.einsum("erd,edf->erf", grouped, expert_up, preferred_element_type=jnp.float32)
    hidden = (jax.nn.silu(gate_part) * up_part).astype(jnp.bfloat16)
    result = jnp.einsum(
        "erf,efd->erd", hidden, expert_down, preferred_element_type=jnp.float32
    ).astype(jnp.bfloat16)
    returned = lax.all_to_all(
        result.reshape(arrived.shape), ("sp", "tp"), split_axis=1, concat_axis=1, tiled=True
    )
    gathered = jnp.dot(
        placement, returned.reshape(-1, model_width), preferred_element_type=jnp.float32
    )
    weighted = gathered.reshape(row_count, pick_count, model_width) * route_weights[:, :, None]
    return jnp.sum(weighted, axis=1)


def body(
    queries,
    key_heads,
    value_heads,
    head_gain,
    residual,
    out_weight,
    norm_gain,
    shared_gate,
    shared_up,
    shared_down,
    expert_gate,
    expert_up,
    expert_down,
    routed_experts,
    route_weights,
):
    head_output = head_norm(stick_breaking(queries, key_heads, value_heads), head_gain)
    token_heads = lax.all_to_all(head_output, "tp", split_axis=0, concat_axis=1, tiled=True)
    branch = jnp.dot(token_heads, out_weight, preferred_element_type=jnp.float32)
    stream = (residual.astype(jnp.float32) + branch).astype(jnp.bfloat16)
    stream_wide = stream.astype(jnp.float32)
    inverse = lax.rsqrt(jnp.mean(stream_wide * stream_wide, axis=1, keepdims=True) + EPSILON)
    expert_input = (stream_wide * inverse * norm_gain).astype(jnp.bfloat16)
    shared_hidden = (
        jax.nn.silu(jnp.dot(expert_input, shared_gate, preferred_element_type=jnp.float32))
        * jnp.dot(expert_input, shared_up, preferred_element_type=jnp.float32)
    ).astype(jnp.bfloat16)
    shared_term = jnp.dot(shared_hidden, shared_down, preferred_element_type=jnp.float32)
    routed = routed_sum(
        expert_input, expert_gate, expert_up, expert_down, routed_experts, route_weights
    )
    return (stream_wide + shared_term + routed).astype(jnp.bfloat16)


def solution(mesh):
    return jax.shard_map(
        body,
        mesh=mesh,
        in_specs=(
            P("sp", "tp"),
            P("sp", "tp"),
            P("sp", "tp"),
            P("tp"),
            P(("sp", "tp"), None),
            P(),
            P(),
            P(),
            P(),
            P(),
            P(("sp", "tp"), None, None),
            P(("sp", "tp"), None, None),
            P(("sp", "tp"), None, None),
            P(("sp", "tp"), None),
            P(("sp", "tp"), None),
        ),
        out_specs=P(("sp", "tp"), None),
        check_vma=False,
    )
```

profile of v0, /device:TPU:0, one launch (start us, length us, event | category | flops | bytes accessed | tf_op | source)
XLA Modules:
  0.0 514.6 jit_solution(18393780882637082508)
XLA Ops:
  9.0 1.7 copy.100
  13.2 39.3 %all-gather.3.cloned.1.call-done = bf16[4096,128]{1,0:T(8,128)(2,1)} async-done(((bf16[512,128]{1,0:T(8,128)(2,1)}), bf16[4096,128]{1,0:T(8,128)(2,1)}) %all-gather.3.cloned.1.call-update) | async-done | bytes 1048592 | tf_op jit(solution)/shard_map/all_gather | solution.py:65
  52.5 5.0 reshape.227
  57.5 5.9 %copy.102 = bf16[8,512,2,64]{1,3,2,0:T(8,128)(2,1)} copy(bf16[8,512,2,64]{3,2,1,0:T(2,128)(2,1)} %reshape.227) | data formatting | bytes 2097152 | tf_op jit(solution)/shard_map/while | solution.py:91
  63.3 30.3 %all-gather.5.cloned.1.call-done = bf16[4096,128]{1,0:T(8,128)(2,1)} async-done(((bf16[512,128]{1,0:T(8,128)(2,1)}), bf16[4096,128]{1,0:T(8,128)(2,1)}) %all-gather.5.cloned.1.call-update) | async-done | bytes 1048592 | tf_op jit(solution)/shard_map/all_gather | solution.py:68
  93.6 5.0 reshape.228
  98.6 4.6 copy.103
  103.2 29.2 %while.14 = (s32[]{:T(128)}, f32[8,512,2]{1,2,0:T(2,128)S(1)}, f32[8,512,2,64]{1,3,2,0:T(8,128)}, s32[]{:T(128)}, s32[1]{0:T(128)}, /*index=5*/bf16[8,512,2,64]{...) while((s32[]{:T(128)}, f32[8,512,2]{1,2,0:T(2,128)S(1)}, ...), condition=%wide.region_6.7_spmd, body=%wide.region_0.6_spmd.sunk | while | flops 217857024 | bytes 41952508 | solution.py:91
  103.4 22.4 %conditional.2 = (f32[1,512,2]{1,2,0:T(2,128)S(1)}, f32[1,512,2,64]{1,3,2,0:T(8,128)S(1)}) conditional(s32[]{:T(128)} %convert_element_type.93, () %tuple.56, (s32[]{:T(128)}, s32[1]{0:T(128)}, bf16[8,512,2,64]{1,3,2,0:T(8,128)(2,1)}, bf16[1,512,2,64]{1,3,2,0:T(8,128)(2,1)}, bf16[8,512,2,64]{1,3,2,0:T(8,128)(2,1)S(1)}) %tuple.57), branch_computations={%region_1.1_spmd, %region_2.5_spmd} | conditional | flops 217857024 | bytes 41419364 | solution.py:86
  103.7 4.0 fusion.1
  107.7 9.6 %fusion.11 = f32[2,512,4,128]{1,2,3,0:T(4,128)S(1)} fusion(f32[2,512,4,128]{1,3,2,0:T(8,128)S(1)} %bitcast.90), kind=kOutput, calls=%fused_computation.17 | output fusion | flops 66584576 | bytes 4194304 | tf_op jit(solution)/shard_map/reduce-window.6
  118.7 2.0 broadcast_add_fusion
  122.2 3.3 fusion.6
  132.5 1.9 multiply_reduce_fusion.1
  135.5 3.5 all-to-all-start
  139.2 4.3 all-to-all-done
  143.5 1.6 multiply_reduce_fusion.2
  145.2 2.7 convolution_convert_fusion.1
  147.9 6.1 %reshape.222 = bf16[2,32,12,2048]{3,2,1,0:T(8,128)(2,1)} reshape(bf16[768,2048]{1,0:T(8,128)(2,1)} %convolution_convert_fusion.1) | data formatting | bytes 6291456 | tf_op jit(solution)/shard_map/reshape | solution.py:120
  154.0 5.5 %copy.109 = bf16[2,32,12,2048]{3,0,2,1:T(2,128)(2,1)S(1)} copy(bf16[2,32,12,2048]{3,2,1,0:T(8,128)(2,1)} %reshape.222) | data formatting | bytes 6291456 | tf_op jit(solution)/shard_map/reshape | solution.py:120
  159.5 230.0 %all_to_all.26 = bf16[2,32,12,2048]{3,0,2,1:T(2,128)(2,1)S(1)} all-to-all(bf16[2,32,12,2048]{3,0,2,1:T(2,128)(2,1)S(1)} %copy.109), channel_id=1, replica_groups=mesh['sp'=8,'tp'=4] {'sp','tp'}, dimensions={1} | all-to-all | bytes 6291456 | tf_op jit(solution)/shard_map/all_to_all | solution.py:121
  389.4 1.7 copy-done.3
  391.1 3.2 fusion.24
  394.3 10.3 %convolution_convert_fusion = bf16[2,384,2048]{2,1,0:T(8,128)(2,1)} fusion(bf16[2,512,2048]{2,1,0:T(8,128)(2,1)} %param.31, f32[2,384,512]{2,1,0:T(8,128)} %fusion.24, bf16[2,2048,512]{2,1,0:T(8,128)(2,1)} %param.30, bf16[2,384,2048]{2,0,1:T(2,128)(2,1)} %bitcast.93), kind=kOutput, calls=%fused_computation.37 | convolution fusion | flops 3225157632 | bytes 16252928 | tf_op jit(solution)/shard_map/erf,efd->erd/dot_general | solution.py:126
  404.6 6.8 %copy.112 = bf16[2,384,2048]{2,0,1:T(2,128)(2,1)} copy(bf16[2,384,2048]{2,1,0:T(8,128)(2,1)} %convolution_convert_fusion) | data formatting | bytes 6291456 | tf_op jit(solution)/shard_map/convert_element_type | solution.py:128
  411.5 4.0 all-to-all-start.2
  415.4 2.1 fusion.59
  417.5 69.5 %all-to-all-done.2 = bf16[2,32,12,2048]{3,0,2,1:T(2,128)(2,1)} async-done(((bf16[2,32,12,2048]{3,0,2,1:T(2,128)(2,1)}), bf16[2,32,12,2048]{3,0,2,1:T(2,128)(2,1)}, u32[]{:S(2)}, u32[]{:S(2)}) %all-to-all-start.2) | async-done | bytes 3145760 | tf_op jit(solution)/shard_map/all_to_all | solution.py:129
  487.0 5.4 %copy.113 = bf16[2,32,12,2048]{3,2,1,0:T(8,128)(2,1)} copy(bf16[2,32,12,2048]{3,0,2,1:T(2,128)(2,1)} %all-to-all-done.2) | data formatting | bytes 6291456 | tf_op jit(solution)/shard_map/all_to_all | solution.py:129
  492.4 6.2 %reshape.226 = bf16[768,2048,1]{1,0,2:T(8,128)(2,1)} reshape(bf16[2,32,12,2048]{3,2,1,0:T(8,128)(2,1)} %copy.113) | data formatting | bytes 6291456 | tf_op jit(solution)/shard_map/reshape | solution.py:133
  498.6 4.8 multiply_reduce_fusion
  503.4 4.2 fusion.29
  (87 shorter events, 16.1 us)
Async XLA Ops:
  6.5 137.0 %copy-start = (bf16[512,2048]{1,0:T(8,128)(2,1)S(1)}, bf16[512,2048]{1,0:T(8,128)(2,1)}, u32[]{:S(2)}) copy-start(bf16[512,2048]{1,0:T(8,128)(2,1)} %param.24) | copy-start | bytes 6291460
  6.5 46.0 %all-gather.3.cloned.1.call-start = ((), (), s32[]{:S(2)}) async-start(), calls=%async_computation.3 | async-start | bytes 1179648 | tf_op jit(solution)/shard_map/all_gather | solution.py:65
  7.3 86.4 %all-gather.5.cloned.1.call-start = ((), (), s32[]{:S(2)}) async-start(), calls=%async_computation.4 | async-start | bytes 1179648 | tf_op jit(solution)/shard_map/all_gather | solution.py:68
  117.3 1.3 copy-start.1
  120.6 1.6 copy-start.2
  132.5 2.1 copy-start.5
  135.5 9.6 %copy-start.4 = (f32[2048]{0:T(1024)S(1)}, f32[2048]{0:T(1024)}, u32[]{:S(2)}) copy-start(f32[2048]{0:T(1024)} %param.25) | copy-start | bytes 24580
  135.5 8.0 %all-to-all-start = ((bf16[4,128,128]{1,2,0:T(8,128)(2,1)}), bf16[4,128,128]{1,2,0:T(8,128)(2,1)S(1)}, u32[]{:S(2)}, u32[]{:S(2)}) async-start(bf16[4,128,128]{1,2,0:T(8,128)(2,1)} %copy.104), calls=%async_computation | async-start | bytes 262144 | tf_op jit(solution)/shard_map/all_to_all | solution.py:157
  159.4 231.7 %copy-start.6 = (bf16[2,2048,512]{2,1,0:T(8,128)(2,1)S(1)}, bf16[2,2048,512]{2,1,0:T(8,128)(2,1)}, u32[]{:S(2)}) copy-start(bf16[2,2048,512]{2,1,0:T(8,128)(2,1)} %param.29) | copy-start | bytes 12582916
  389.4 1.7 copy-start.3
  411.5 75.5 %all-to-all-start.2 = ((bf16[2,32,12,2048]{3,0,2,1:T(2,128)(2,1)}), bf16[2,32,12,2048]{3,0,2,1:T(2,128)(2,1)}, u32[]{:S(2)}, u32[]{:S(2)}) async-start(bf16[2,32,12,2048]{3,0,2,1:T(2,128)(2,1)} %bitcast.91), calls=%async_computation.2 | async-start | bytes 6291456 | tf_op jit(solution)/shard_map/all_to_all | solution.py:129
  492.4 6.2 %copy-start.7 = (f32[128,4]{0,1:T(4,128)S(1)}, f32[128,4]{0,1:T(4,128)}, u32[]{:S(2)}) copy-start(f32[128,4]{0,1:T(4,128)} %param.33) | copy-start | bytes 6148
Sparse Core Ops, SparseCore 0:
  9.5 42.9 all-gather.2
  54.6 38.9 all-gather.4
where the time goes:
time: 520 us; the launch traced here: 515 us
  blocking collectives  230 us (44%)
  waiting for transfers between devices  145 us (28%)
  local copies, waits for them, and re-layouts  64.9 us (12%)
  matrix products  33.1 us (6%)
  other arithmetic  19.7 us (4%)
  between operations  13.8 us (3%)
  starting transfers between devices  7.45 us (1%)
    all_to_all x1, blocking collectives, routed_sum(): lax.all_to_all(outgoing, ('sp', 'tp'), split_axis=1, concat_axis=1, tiled...  230 us
    all_to_all x1, waiting for transfers between devices, routed_sum(): lax.all_to_all(result.reshape(arrived.shape), ('sp', 'tp'), split_axis=1,...  69.5 us
    all_gather x1, waiting for transfers between devices, stick_breaking(): lax.all_gather(key_heads, 'sp', axis=0, tiled=True)  39.3 us
    all_gather x1, waiting for transfers between devices, stick_breaking(): lax.all_gather(value_heads, 'sp', axis=0, tiled=True)  30.3 us
    reshape x2, local copies, waits for them, and re-layouts, routed_sum(): outgoing.reshape(local_experts, device_count, capacity, model_width)  11.5 us
    another operation x4, other arithmetic  10.9 us
    while x2, local copies, waits for them, and re-layouts, stick_breaking(): totals, partials = lax.fori_loop(0, key_piece.shape[0], add_one, initial)  10.5 us
  transfers between devices with their start and end apart: 4, of which 4 were waited for; matrix products, arithmetic and copies ran while one was open for 4% of the time, Pallas kernels for 0%

commit v1 on v0

--- a/solution.py
+++ b/solution.py
@@ -126,8 +126,16 @@
     result = jnp.einsum(
         "erf,efd->erd", hidden, expert_down, preferred_element_type=jnp.float32
     ).astype(jnp.bfloat16)
-    returned = lax.all_to_all(
-        result.reshape(arrived.shape), ("sp", "tp"), split_axis=1, concat_axis=1, tiled=True
+    returned = jnp.concatenate(
+        lax.all_to_all(
+            jnp.stack(
+                jnp.split(result.reshape(arrived.shape), lax.axis_size(("sp", "tp")), axis=1)
+            ),
+            ("sp", "tp"),
+            0,
+            0,
+        ),
+        axis=1,
     )
     gathered = jnp.dot(
         placement, returned.reshape(-1, model_width), preferred_element_type=jnp.float32

time: 520 us -> 539 us (1.037)
  local copies, waits for them, and re-layouts: 64.9 us -> 85.6 us
    unnamed x14 -> x49, local copies, waits for them, and re-layouts: 4.18 us -> 25.9 us
    another operation x4 -> x6, local copies, waits for them, and re-layouts: 0.25 us -> 7.12 us  [the longest x1 6.17 us: routed_sum(): returned.reshape(-1, model_width)]
    all_to_all x1 -> x0, local copies, waits for them, and re-layouts: 5.41 us -> none  [routed_sum(): lax.all_to_all(result.reshape(arrived.shape), ('sp', 'tp'), split_axis=1,...]
  transfers between devices with their start and end apart: 4 -> 4, of which waited for: 4 -> 4; matrix products, arithmetic and copies ran while one was open for 4% -> 3% of each run, Pallas kernels for 0% -> 0%
where the time goes in v1:
time: 539 us; the launch traced here: 534 us
  blocking collectives  230 us (43%)
  waiting for transfers between devices  146 us (27%)
  local copies, waits for them, and re-layouts  85.6 us (16%)
  matrix products  30.1 us (6%)
  other arithmetic  19.7 us (4%)
  between operations  13.8 us (3%)
  starting transfers between devices  7.4 us (1%)
    all_to_all x1, blocking collectives, routed_sum(): lax.all_to_all(outgoing, ('sp', 'tp'), split_axis=1, concat_axis=1, tiled...  230 us
    all_to_all x1, waiting for transfers between devices, routed_sum(): lax.all_to_all(jnp.stack(jnp.split(result.reshape(arrived.shape), lax.axi...  71.1 us
    all_gather x1, waiting for transfers between devices, stick_breaking(): lax.all_gather(key_heads, 'sp', axis=0, tiled=True)  39.3 us
    all_gather x1, waiting for transfers between devices, stick_breaking(): lax.all_gather(value_heads, 'sp', axis=0, tiled=True)  30.3 us
    unnamed x49, local copies, waits for them, and re-layouts  25.9 us
    reshape x2, local copies, waits for them, and re-layouts, routed_sum(): outgoing.reshape(local_experts, device_count, capacity, model_width)  11.5 us
    another operation x4, other arithmetic  10.9 us
  transfers between devices with their start and end apart: 4, of which 4 were waited for; matrix products, arithmetic and copies ran while one was open for 3% of the time, Pallas kernels for 0%

profile of v1, /device:TPU:0, one launch (start us, length us, event | category | flops | bytes accessed | tf_op | source)
XLA Modules:
  0.0 533.8 jit_solution(12415297107952839414)
XLA Ops:
  9.0 1.7 copy.132
  13.2 39.3 %all-gather.3.cloned.1.call-done = bf16[4096,128]{1,0:T(8,128)(2,1)} async-done(((bf16[512,128]{1,0:T(8,128)(2,1)}), bf16[4096,128]{1,0:T(8,128)(2,1)}) %all-gather.3.cloned.1.call-update) | async-done | bytes 1048592 | tf_op jit(solution)/shard_map/all_gather | solution.py:65
  52.5 5.0 reshape.227
  57.5 5.9 %copy.134 = bf16[8,512,2,64]{1,3,2,0:T(8,128)(2,1)} copy(bf16[8,512,2,64]{3,2,1,0:T(2,128)(2,1)} %reshape.227) | data formatting | bytes 2097152 | tf_op jit(solution)/shard_map/while | solution.py:91
  63.3 30.3 %all-gather.5.cloned.1.call-done = bf16[4096,128]{1,0:T(8,128)(2,1)} async-done(((bf16[512,128]{1,0:T(8,128)(2,1)}), bf16[4096,128]{1,0:T(8,128)(2,1)}) %all-gather.5.cloned.1.call-update) | async-done | bytes 1048592 | tf_op jit(solution)/shard_map/all_gather | solution.py:68
  93.6 5.0 reshape.228
  98.6 4.6 copy.135
  103.2 29.2 %while.14 = (s32[]{:T(128)}, f32[8,512,2]{1,2,0:T(2,128)S(1)}, f32[8,512,2,64]{1,3,2,0:T(8,128)}, s32[]{:T(128)}, s32[1]{0:T(128)}, /*index=5*/bf16[8,512,2,64]{...) while((s32[]{:T(128)}, f32[8,512,2]{1,2,0:T(2,128)S(1)}, ...), condition=%wide.region_6.7_spmd, body=%wide.region_0.6_spmd.sunk | while | flops 217857024 | bytes 41952508 | solution.py:91
  103.4 22.4 %conditional.2 = (f32[1,512,2]{1,2,0:T(2,128)S(1)}, f32[1,512,2,64]{1,3,2,0:T(8,128)S(1)}) conditional(s32[]{:T(128)} %convert_element_type.93, () %tuple.56, (s32[]{:T(128)}, s32[1]{0:T(128)}, bf16[8,512,2,64]{1,3,2,0:T(8,128)(2,1)}, bf16[1,512,2,64]{1,3,2,0:T(8,128)(2,1)}, bf16[8,512,2,64]{1,3,2,0:T(8,128)(2,1)S(1)}) %tuple.57), branch_computations={%region_1.1_spmd, %region_2.5_spmd} | conditional | flops 217857024 | bytes 41419364 | solution.py:86
  103.7 4.0 fusion.1
  107.7 9.6 %fusion.11 = f32[2,512,4,128]{1,2,3,0:T(4,128)S(1)} fusion(f32[2,512,4,128]{1,3,2,0:T(8,128)S(1)} %bitcast.221), kind=kOutput, calls=%fused_computation.17 | output fusion | flops 66584576 | bytes 4194304 | tf_op jit(solution)/shard_map/reduce-window.6
  117.3 1.3 copy-done.2
  118.7 2.0 broadcast_add_fusion
  122.2 3.3 fusion.6
  132.5 1.9 multiply_reduce_fusion.1
  135.5 3.3 all-to-all-start
  139.1 4.3 all-to-all-done
  143.4 1.6 multiply_reduce_fusion.2
  145.0 2.7 convolution_convert_fusion.1
  147.8 6.1 %reshape.222 = bf16[2,32,12,2048]{3,2,1,0:T(8,128)(2,1)} reshape(bf16[768,2048]{1,0:T(8,128)(2,1)} %convolution_convert_fusion.1) | data formatting | bytes 6291456 | tf_op jit(solution)/shard_map/reshape | solution.py:120
  153.8 5.5 %copy.141 = bf16[2,32,12,2048]{3,0,2,1:T(2,128)(2,1)S(1)} copy(bf16[2,32,12,2048]{3,2,1,0:T(8,128)(2,1)} %reshape.222) | data formatting | bytes 6291456 | tf_op jit(solution)/shard_map/reshape | solution.py:120
  159.3 230.0 %all_to_all.26 = bf16[2,32,12,2048]{3,0,2,1:T(2,128)(2,1)S(1)} all-to-all(bf16[2,32,12,2048]{3,0,2,1:T(2,128)(2,1)S(1)} %copy.141), channel_id=1, replica_groups=mesh['sp'=8,'tp'=4] {'sp','tp'}, dimensions={1} | all-to-all | bytes 6291456 | tf_op jit(solution)/shard_map/all_to_all | solution.py:121
  389.3 1.7 copy-done.4
  391.0 2.0 fusion.24
  393.0 9.9 %convolution_convert_fusion = bf16[2,384,2048]{2,1,0:T(8,128)(2,1)} fusion(bf16[2,512,2048]{2,1,0:T(8,128)(2,1)} %param.31, f32[2,384,512]{2,1,0:T(8,128)S(1)} %fusion.24, bf16[2,2048,512]{2,1,0:T(8,128)(2,1)} %param.30, bf16[2,384,2048]{2,0,1:T(2,128)(2,1)} %bitcast.255), kind=kOutput, calls=%fused_computation.37 | convolution fusion | flops 3225157632 | bytes 16252928 | tf_op jit(solution)/shard_map/erf,efd->erd/dot_general | solution.py:126
  402.9 5.1 copy.144
  430.5 4.0 all-to-all-start.2
  435.0 71.1 %all-to-all-done.2 = bf16[32,2,1,12,2048]{4,1,3,2,0:T(2,128)(2,1)} async-done(((bf16[32,2,1,12,2048]{4,1,3,2,0:T(2,128)(2,1)}), bf16[32,2,1,12,2048]{4,1,3,2,0:T(2,128)(2,1)}, u32[]{:S(2)}, u32[]{:S(2)}) %all-to-all-start.2) | async-done | bytes 3145760 | tf_op jit(solution)/shard_map/all_to_all | solution.py:130
  506.1 5.4 %copy.145 = bf16[2,32,1,12,2048]{4,3,1,0,2:T(8,128)(2,1)} copy(bf16[2,32,1,12,2048]{4,0,3,2,1:T(2,128)(2,1)} %bitcast.52) | data formatting | bytes 6291456 | tf_op jit(solution)/shard_map/reshape | solution.py:129
  511.5 6.2 %reshape.226 = bf16[768,2048,1]{1,0,2:T(8,128)(2,1)} reshape(bf16[2,32,1,12,2048]{4,3,1,0,2:T(8,128)(2,1)} %copy.145) | data formatting | bytes 6291456 | tf_op jit(solution)/shard_map/reshape;reshape | solution.py:141
  517.7 4.9 multiply_reduce_fusion
  522.6 4.2 fusion.29
  (123 shorter events, 37.7 us)
Async XLA Ops:
  6.5 136.9 %copy-start = (bf16[512,2048]{1,0:T(8,128)(2,1)S(1)}, bf16[512,2048]{1,0:T(8,128)(2,1)}, u32[]{:S(2)}) copy-start(bf16[512,2048]{1,0:T(8,128)(2,1)} %param.24) | copy-start | bytes 6291460
  6.5 46.0 %all-gather.3.cloned.1.call-start = ((), (), s32[]{:S(2)}) async-start(), calls=%async_computation.3 | async-start | bytes 1179648 | tf_op jit(solution)/shard_map/all_gather | solution.py:65
  7.3 86.4 %all-gather.5.cloned.1.call-start = ((), (), s32[]{:S(2)}) async-start(), calls=%async_computation.4 | async-start | bytes 1179648 | tf_op jit(solution)/shard_map/all_gather | solution.py:68
  117.3 1.3 copy-start.2
  120.6 1.6 copy-start.3
  132.5 2.1 copy-start.7
  134.4 10.6 %copy-start.6 = (f32[2048]{0:T(1024)S(1)}, f32[2048]{0:T(1024)}, u32[]{:S(2)}) copy-start(f32[2048]{0:T(1024)} %param.25) | copy-start | bytes 24580
  135.5 7.9 %all-to-all-start = ((bf16[4,128,128]{1,2,0:T(8,128)(2,1)}), bf16[4,128,128]{1,2,0:T(8,128)(2,1)S(1)}, u32[]{:S(2)}, u32[]{:S(2)}) async-start(bf16[4,128,128]{1,2,0:T(8,128)(2,1)} %copy.136), calls=%async_computation | async-start | bytes 262144 | tf_op jit(solution)/shard_map/all_to_all | solution.py:165
  159.3 231.7 %copy-start.8 = (bf16[2,2048,512]{2,1,0:T(8,128)(2,1)S(1)}, bf16[2,2048,512]{2,1,0:T(8,128)(2,1)}, u32[]{:S(2)}) copy-start(bf16[2,2048,512]{2,1,0:T(8,128)(2,1)} %param.29) | copy-start | bytes 12582916
  389.3 1.7 copy-start.4
  430.5 4.0 copy-start.5
  430.5 75.6 %all-to-all-start.2 = ((bf16[32,2,1,12,2048]{4,1,3,2,0:T(2,128)(2,1)}), bf16[32,2,1,12,2048]{4,1,3,2,0:T(2,128)(2,1)}, u32[]{:S(2)}, u32[]{:S(2)}) async-start(bf16[32,2,1,12,2048]{4,1,3,2,0:T(2,128)(2,1)} %fusion.51), calls=%async_computation.2 | async-start | bytes 6291456 | tf_op jit(solution)/shard_map/all_to_all | solution.py:130
  511.5 6.2 %copy-start.9 = (f32[128,4]{0,1:T(4,128)S(1)}, f32[128,4]{0,1:T(4,128)}, u32[]{:S(2)}) copy-start(f32[128,4]{0,1:T(4,128)} %param.33) | copy-start | bytes 6148
  517.7 9.1 %copy-start.1 = (bf16[512,2048]{1,0:T(8,128)(2,1)S(1)}, bf16[512,2048]{1,0:T(8,128)(2,1)}, u32[]{:S(2)}) copy-start(bf16[512,2048]{1,0:T(8,128)(2,1)} %param.24) | copy-start | bytes 6291460
Sparse Core Ops, SparseCore 0:
  9.5 42.9 all-gather.2
  54.6 38.9 all-gather.4
